TPU v7x, 256 devices: a whole 4x4x8 slice. The times are simulated.
256 devices in a mesh: ep: 128 (over z, y, x), tp: 2 (over core).
Axes of the slice: x: 4, y: 4, z: 8, core: 2. Of those that a mesh axis runs over, the one named last changes fastest.
Arguments:
- tokens: bfloat16 [2048, 1024], P('ep'), may hold values from -6 to 6
- mixer_gain: float32 [1024], replicated, may hold values from 0.1 to 1.9
- query_weight: bfloat16 [1024, 1024], P(None, 'tp'), may hold values from -0.1875 to 0.1875
- key_weight: bfloat16 [1024, 256], P(None, 'tp'), may hold values from -0.1875 to 0.1875
- value_weight: bfloat16 [1024, 256], P(None, 'tp'), may hold values from -0.1875 to 0.1875
- head_lambda: float32 [8], P('tp'), may hold values from 0.3 to 0.8
- head_gain: float32 [128], replicated, may hold values from 0.1 to 1.9
- out_weight: bfloat16 [1024, 1024], P('tp'), may hold values from -0.1875 to 0.1875
- cache_keys: bfloat16 [2048, 1024, 256], P('ep', None, 'tp'), may hold values from -700 to 700
- cache_values: bfloat16 [2048, 1024, 256], P('ep', None, 'tp'), may hold values from -6 to 6
- seq_lengths: int32 [2048], P('ep'), may hold values from 2 to 1024, as said below
- channel_gain: float32 [1024], replicated, may hold values from 0.1 to 1.9
- expert_ids: int32 [2048, 6], P('ep'), may hold values from 0 to 127, all different within a row; in each aligned block of 16 rows (0 to 15, 16 to 31, ...) at most 2 rows name the same one
- expert_shares: bfloat16 [2048, 6], P('ep'), may hold values from 0.19921875 to 1
- expert_gate: bfloat16 [128, 1024, 256], P('ep', None, 'tp'), may hold values from -0.1875 to 0.1875
- expert_up: bfloat16 [128, 1024, 256], P('ep', None, 'tp'), may hold values from -0.1875 to 0.1875
- expert_down: bfloat16 [128, 256, 1024], P('ep', 'tp'), may hold values from -0.375 to 0.375
- dense_gate: bfloat16 [1024, 4096], P('tp', 'ep'), may hold values from -0.1875 to 0.1875
- dense_up: bfloat16 [1024, 4096], P('tp', 'ep'), may hold values from -0.1875 to 0.1875
- dense_down: bfloat16 [4096, 1024], P('ep', 'tp'), may hold values from -0.1875 to 0.1875
- branch_gate: float32 [1024], replicated, may hold values from -0.1875 to 0.1875
Outputs:
- layer_out: bfloat16 [2048, 1024], P('ep', 'tp')
Inputs may be any that keep to these rules, and one draw needn't show every extreme that they name: `expert_ids`: each row names 6 different experts; among the 16 rows of one index of ep no expert is named by more than 2 rows. `seq_lengths`: some sequence has all 1024 positions live.
All inputs are finite; a program needn't handle non-finite values.
Results may differ from a plain program's by a relative error of at most 0.017.
The roundings to bfloat16 on the way count: a program that leaves them out, or rounds other values in their place, can miss the bound.
Values may be sent and summed in bfloat16 or wider, within the bound.
No kernel may reach another device: no remote copies, remote signals or barrier semaphores. Data moves between devices by JAX's collectives and lax.ppermute only.
A program may use at most 64 MiB of HBM per device.

v0:
```python
import math
import jax
import jax.numpy as jnp
from jax import lax
from jax.experimental import pallas as pl
from jax.experimental.pallas import tpu as pltpu
from jax.sharding import Mesh
from jax.sharding import PartitionSpec as P

HD = 64
NORM_EPS = 1e-06
HEAD_EPS = 1e-05
THETA = 500000.0
LAMBDA_BASE = 0.2
F32 = jnp.float32
BF16 = jnp.bfloat16
BLOCKS = 4


def attention_body(
    lens_hbm, lam_hbm, tokens_hbm, mixer_hbm, wq_hbm, wk_hbm, wv_hbm, head_gain_hbm, wo_hbm, keys_hbm, values_hbm, out,
    lens, lam, tokens, mixer_gain, head_gain, wq, wk, wv, wo, keys, values, qrows, scores, mixed, ssem, wsem, ksem, vsem,
):
    seqs, span, width = keys.shape
    heads = lam.shape[0]
    rows = seqs * heads
    block = span // BLOCKS
    half_span, half_seqs = span // 2, seqs // 2
    weights = [
        pltpu.make_async_copy(src, dst, wsem.at[i])
        for i, (src, dst) in enumerate(((wk_hbm, wk), (wq_hbm, wq), (wv_hbm, wv), (wo_hbm, wo)))
    ]
    key_copies = [
        pltpu.make_async_copy(
            keys_hbm.at[:, pl.ds(b * half_span, half_span), :], keys.at[:, pl.ds(b * half_span, half_span), :], ksem.at[b]
        )
        for b in range(2)
    ]
    value_copies = [
        pltpu.make_async_copy(
            values_hbm.at[pl.ds(b * half_seqs, half_seqs)], values.at[pl.ds(b * half_seqs, half_seqs)], vsem.at[b]
        )
        for b in range(2)
    ]
    small = [
        pltpu.make_async_copy(src, dst, ssem.at[i])
        for i, (src, dst) in enumerate(
            (
                (tokens_hbm, tokens), (mixer_hbm, mixer_gain), (lens_hbm, lens), (lam_hbm, lam),
                (head_gain_hbm, head_gain),
            )
        )
    ]
    for copy in small + weights[:3] + key_copies:
        copy.start()
    for copy in small[:2]:
        copy.wait()

    resid = tokens[...].astype(F32)
    mean_square = jnp.mean(resid * resid, axis=-1, keepdims=True)
    normed = (resid * lax.rsqrt(mean_square + NORM_EPS) * mixer_gain[...]).astype(BF16)

    weights[0].wait()
    key_raw = jnp.dot(normed, wk[...], preferred_element_type=F32)
    weights[1].wait()
    query_raw = jnp.dot(normed, wq[...], preferred_element_type=F32)
    for copy in value_copies + weights[3:]:
        copy.start()
    for copy in small[2:]:
        copy.wait()

    row = lax.broadcasted_iota(jnp.int32, (seqs, width), 0)
    lane = lax.broadcasted_iota(jnp.int32, (seqs, width), 1)
    position = jnp.zeros((seqs, width), jnp.int32)
    for s in range(seqs):
        position = jnp.where(row == s, lens[s], position)
    half = HD // 2
    frequency = jnp.exp((lane % half).astype(F32) * (-2.0 / HD * math.log(THETA)))
    angles = position.astype(F32) * frequency
    first = lane % HD < half
    cos_vals = jnp.cos(angles)
    sin_vals = jnp.sin(angles)
    sin_vals = jnp.where(first, -sin_vals, sin_vals)

    def rotate(tile):
        swapped = jnp.where(first, pltpu.roll(tile, width - half, 1), pltpu.roll(tile, half, 1))
        return (tile * cos_vals + swapped * sin_vals).astype(BF16).astype(F32)

    column = lax.broadcasted_iota(jnp.int32, (1, width), 1)
    owner = column % rows // heads
    limit = jnp.zeros((1, width), jnp.int32)
    for s in range(seqs):
        limit = jnp.where(owner == s, lens[s], limit)
    mult = jnp.ones((1, width), F32)
    for j in range(heads):
        mult = jnp.where(column == rows + column % rows // heads * heads + j, lam[j], mult)

    knew = rotate(key_raw).astype(BF16)
    for j in range(heads):
        tile = rotate(query_raw[:, j * width : (j + 1) * width]) * HD ** (-0.5)
        qrows[pl.ds(j, seqs, stride=heads), :] = jnp.where(lane < HD, tile, 0.0)
        qrows[pl.ds(rows + j, seqs, stride=heads), :] = jnp.where(lane < HD, 0.0, tile)
    qcols = jnp.transpose(qrows[...])
    query = jnp.concatenate([jnp.where(owner == s, qcols, 0.0).astype(BF16) for s in range(seqs)], axis=0)
    weights[2].wait()
    vnew = jnp.dot(normed, wv[...], preferred_element_type=F32).astype(BF16).astype(F32)
    for j in range(heads):
        mixed[pl.ds(j, seqs, stride=heads), :] = vnew

    new_row = jnp.concatenate([knew[s : s + 1, :] for s in range(seqs)], axis=1)
    new_row = jnp.broadcast_to(new_row, (16, seqs * width))
    new_score = jnp.dot(new_row, query, preferred_element_type=F32)[:1]
    peak = new_score
    for b in range(BLOCKS):
        if b * block % half_span == 0:
            key_copies[b * block // half_span].wait()
        past = jnp.concatenate([keys[s, pl.ds(b * block, block), :] for s in range(seqs)], axis=1)
        score = jnp.dot(past, query, preferred_element_type=F32)
        place = lax.broadcasted_iota(jnp.int32, (block, width), 0) + b * block
        score = jnp.where(place < limit, score, -jnp.inf)
        scores[pl.ds(b * block, block), :] = score
        peak = jnp.maximum(peak, jnp.max(score, axis=0, keepdims=True))
    expo = jnp.exp(scores[...] - peak)
    expo_new = jnp.exp(new_score - peak)
    factor = mult / (jnp.sum(expo, axis=0, keepdims=True) + expo_new)
    scaled = expo * factor
    weight = jnp.transpose(scaled - pltpu.roll(scaled, rows, 1))[:rows].astype(BF16)
    scaled_new = jnp.broadcast_to(expo_new * factor, (width, width))
    weight_new = jnp.transpose(scaled_new - pltpu.roll(scaled_new, rows, 1))[:rows].astype(BF16).astype(F32)
    pair = 8 // heads
    part = lax.broadcasted_iota(jnp.int32, (8, width), 0) // heads
    for g in range(seqs // pair):
        group = jnp.zeros((8, width), F32)
        for i in range(pair):
            s = g * pair + i
            if s % half_seqs == 0:
                value_copies[s // half_seqs].wait()
            own = jnp.dot(weight[g * 8 : g * 8 + 8], values[s], preferred_element_type=F32)
            group = jnp.where(part == i, own, group)
        where = pl.ds(g * 8, 8)
        mixed[where, :] = group + weight_new[g * 8 : g * 8 + 8] * mixed[where, :]
    mix = mixed[...]
    mix_square = jnp.mean(mix * mix, axis=-1, keepdims=True)
    mixed[...] = mix * lax.rsqrt(mix_square + HEAD_EPS) * head_gain[...] * (1.0 - LAMBDA_BASE)
    head_out = jnp.concatenate([mixed[pl.ds(j, seqs, stride=heads), :] for j in range(heads)], axis=1)
    weights[3].wait()
    out[...] = jnp.dot(head_out.astype(BF16), wo[...], preferred_element_type=F32)


def attention(lens, lam, tokens, mixer_gain, wq, wk, wv, head_gain, wo, cache_keys, cache_values):
    seqs, model_width = tokens.shape
    span, width = cache_keys.shape[1:]
    heads = lam.shape[0]
    vmem = pl.BlockSpec(memory_space=pltpu.VMEM)
    hbm = pl.BlockSpec(memory_space=pltpu.HBM)
    operands = (lens, lam, tokens, mixer_gain, wq, wk, wv, head_gain, wo, cache_keys, cache_values)
    operands = [pltpu.with_memory_space_constraint(x, pltpu.HBM) for x in operands]
    return pl.pallas_call(
        attention_body,
        out_shape=pltpu.VMEM((seqs, model_width), F32),
        in_specs=[hbm] * 11,
        out_specs=vmem,
        scratch_shapes=[
            pltpu.SMEM(lens.shape, jnp.int32),
            pltpu.SMEM(lam.shape, F32),
            pltpu.VMEM(tokens.shape, BF16),
            pltpu.VMEM(mixer_gain.shape, F32),
            pltpu.VMEM(head_gain.shape, F32),
            pltpu.VMEM(wq.shape, BF16),
            pltpu.VMEM(wk.shape, BF16),
            pltpu.VMEM(wv.shape, BF16),
            pltpu.VMEM(wo.shape, BF16),
            pltpu.VMEM((seqs, span, width), BF16),
            pltpu.VMEM((seqs, span, width), BF16),
            pltpu.VMEM((2 * seqs * heads, width), F32),
            pltpu.VMEM((span, width), F32),
            pltpu.VMEM((seqs * heads, width), F32),
            pltpu.SemaphoreType.DMA((5,)),
            pltpu.SemaphoreType.DMA((4,)),
            pltpu.SemaphoreType.DMA((2,)),
            pltpu.SemaphoreType.DMA((2,)),
        ],
        compiler_params=pltpu.CompilerParams(vmem_limit_bytes=20 * 1024 * 1024),
        cost_estimate=pl.CostEstimate(flops=10**9, bytes_accessed=12 * 1024 * 1024, transcendentals=10**6),
        name="attention",
    )(*operands)


EP = ("zh", "zl", "yh", "yl", "xh", "xl")
SMEM = pl.BlockSpec(memory_space=pltpu.SMEM)
VMEM = pl.BlockSpec(memory_space=pltpu.VMEM)


def call(body, out_shape, in_specs, scratch=(), flops=10**8):
    return pl.pallas_call(
        body,
        out_shape=out_shape,
        in_specs=in_specs,
        out_specs=jax.tree.map(lambda _: VMEM, out_shape),
        scratch_shapes=list(scratch),
        compiler_params=pltpu.CompilerParams(vmem_limit_bytes=12 * 1024 * 1024),
        cost_estimate=pl.CostEstimate(flops=flops, bytes_accessed=2 * 1024 * 1024, transcendentals=10**5),
    )


def mid_body(core, tokens, own, other, channel_gain, ids, shares, branch_gate, send, mid, pick, gate, slab):
    seqs, model_width = tokens.shape
    peers, lines, width = send.shape
    chunks = model_width // width
    summed = (tokens[...].astype(F32) + (own[...] + other[...])).astype(BF16)
    mid[...] = summed
    wide = summed.astype(F32)
    mean_square = jnp.mean(wide * wide, axis=-1, keepdims=True)
    ffn = (wide * lax.rsqrt(mean_square + NORM_EPS) * channel_gain[...]).astype(BF16)
    logit = jnp.sum(ffn.astype(F32) * branch_gate[...], axis=-1, keepdims=True)
    gate[...] = jnp.broadcast_to(jax.nn.sigmoid(logit), gate.shape)

    peer = lax.broadcasted_iota(jnp.int32, (seqs, peers), 1)
    row = lax.broadcasted_iota(jnp.int32, (seqs, peers), 0)
    share = jnp.zeros((seqs, peers), F32)
    picked = jnp.zeros((seqs, peers), F32)
    for k in range(ids.shape[1]):
        named = ids[:, k : k + 1] == peer
        picked = jnp.where(named, 1.0, picked)
        share = jnp.where(named, shares[:, k : k + 1].astype(F32), share)
    above = lax.broadcasted_iota(jnp.int32, (seqs, seqs), 0) >= lax.broadcasted_iota(jnp.int32, (seqs, seqs), 1)
    rank = jnp.dot(above.astype(BF16), picked.astype(BF16), preferred_element_type=F32)
    placed = (picked > 0.0) & (rank == (core[0] + 1).astype(F32))
    pick[...] = jnp.where(placed, share, 0.0).astype(BF16)
    dense = row == 2 * member(peer) + core[0]
    for r, chosen in enumerate((placed, dense)):
        lines_out = lax.dot_general(
            chosen.astype(F32).astype(BF16), ffn, (((0,), (0,)), ((), ())), preferred_element_type=F32
        )
        for k in range(chunks):
            slab[pl.ds(r * chunks + k, peers, stride=lines), :] = lines_out[:, k * width : (k + 1) * width]
    send[...] = slab[...].reshape(send.shape).astype(BF16)


def member(peer):
    return (peer // 16 % 2) * 4 + (peer // 4 % 2) * 2 + peer % 2


def unpack(slab, first, chunks, lines):
    peers = slab.shape[0] // lines
    return [slab[pl.ds(first + k, peers, stride=lines), :].astype(BF16) for k in range(chunks)]


def experts_body(
    core, arrived, gate_own, gate_other, up_own, up_other, dense_own, dense_other, down_own, down_other, out, slab,
    down_late, sem,
):
    late = pltpu.make_async_copy(down_other, down_late, sem)
    late.start()
    peers, lines, width = arrived.shape
    chunks = lines // 2
    slab[...] = arrived[...].reshape(slab.shape).astype(F32)
    routed = jnp.concatenate(unpack(slab, 0, chunks, lines), axis=1)
    tokens = unpack(slab, chunks, chunks, lines)
    low, high = jnp.concatenate(tokens[: chunks // 2], axis=1), jnp.concatenate(tokens[chunks // 2 :], axis=1)
    is_first = core[0] == 0
    blocks, stacked, half_width = dense_own.shape
    units = stacked // 3

    def part(ref, i):
        return ref[:, i * units : (i + 1) * units, :].reshape(blocks * units, half_width)

    mine, theirs = jnp.where(is_first, low, high), jnp.where(is_first, high, low)

    def project(i):
        dims = (((1,), (1,)), ((), ()))
        return lax.dot_general(mine, part(dense_own, i), dims, preferred_element_type=F32) + lax.dot_general(
            theirs, part(dense_other, i), dims, preferred_element_type=F32
        )

    hidden = (jax.nn.silu(project(0)) * project(1)).astype(BF16)
    sum_own = jnp.dot(hidden, part(dense_own, 2), preferred_element_type=F32)
    sum_other = jnp.dot(hidden, part(dense_other, 2), preferred_element_type=F32)
    halves = (jnp.where(is_first, sum_own, sum_other), jnp.where(is_first, sum_other, sum_own))
    for h, value in enumerate(halves):
        for k in range(chunks // 2):
            where = pl.ds(chunks + h * chunks // 2 + k, peers, stride=lines)
            slab[where, :] = value[:, k * width : (k + 1) * width]
    result = jnp.zeros((peers, chunks * width), F32)
    for w_gate, w_up, w_down in ((gate_own, up_own, down_own), (gate_other, up_other, down_late)):
        gate_part = jnp.dot(routed, w_gate[0], preferred_element_type=F32)
        up_part = jnp.dot(routed, w_up[0], preferred_element_type=F32)
        hidden = (jax.nn.silu(gate_part) * up_part).astype(BF16)
        if w_down is down_late:
            late.wait()
        result = result + jnp.dot(hidden, w_down[0], preferred_element_type=F32)
    for k in range(chunks):
        slab[pl.ds(k, peers, stride=lines), :] = result[:, k * width : (k + 1) * width]
    out[...] = slab[...].reshape(out.shape).astype(BF16)


def combine_body(core, returned, pick, gate, mid, keep, send, slab):
    peers, lines, width = returned.shape
    chunks = lines // 2
    seqs = pick.shape[0]
    slab[...] = returned[...].reshape(slab.shape).astype(F32)
    peer = lax.broadcasted_iota(jnp.int32, (seqs, peers), 1)
    row = lax.broadcasted_iota(jnp.int32, (seqs, peers), 0)
    dense = (row == 2 * member(peer) + core[0]).astype(F32).astype(BF16)
    routed = jnp.dot(pick[...], jnp.concatenate(unpack(slab, 0, chunks, lines), axis=1), preferred_element_type=F32)
    branch = jnp.dot(dense, jnp.concatenate(unpack(slab, chunks, chunks, lines), axis=1), preferred_element_type=F32)
    total = routed + gate[:, :1] * branch
    half = chunks * width // 2
    is_first = core[0] == 0
    low, high = total[:, :half], total[:, half:]
    resid = mid[...].astype(F32)
    keep[...] = jnp.where(is_first, resid[:, :half] + low, resid[:, half:] + high)
    send[...] = jnp.where(is_first, high, low)


def swap(value, axis):
    return lax.ppermute(value, axis, [(0, 1), (1, 0)])


def layer(
    tokens, mixer_gain, query_weight, key_weight, value_weight, head_lambda, head_gain, out_weight,
    cache_keys, cache_values, seq_lengths, channel_gain, expert_ids, expert_shares,
    expert_gate, expert_up, expert_down, dense_gate, dense_up, dense_down, branch_gate,
):
    seqs, model_width = tokens.shape
    peers = lax.axis_size(EP)
    width = 2 * HD
    lines = 2 * model_width // width
    half = model_width // 2
    core = lax.axis_index("tp").astype(jnp.int32).reshape(1)
    sds = jax.ShapeDtypeStruct
    slab = pltpu.VMEM((peers * lines, width), F32)

    gate_other, up_other, down_other = (swap(w, "tp") for w in (expert_gate, expert_up, expert_down))

    first = jnp.concatenate([dense_gate.T, dense_up.T, dense_down], axis=0)[None]
    second = swap(first, "zl")
    own = attention(
        seq_lengths, head_lambda, tokens, mixer_gain.reshape(1, -1), query_weight, key_weight, value_weight,
        head_gain.reshape(1, -1), out_weight, cache_keys, cache_values,
    )
    other = swap(own, "tp")
    pair = jnp.concatenate([first, second], axis=0)
    pair_y = swap(pair, "yl")
    pair_x = swap(pair, "xl")
    cut_y, cut_x = pair_y[:1], pair_x[1:]
    corner_x = swap(cut_y, "xl")
    corner_y = swap(cut_x, "yl")
    gathered = jnp.concatenate([pair, pair_y, pair_x, corner_x, corner_y], axis=0)
    gathered_other = swap(gathered, "tp")
    middle = call(
        mid_body,
        (
            sds((peers, lines, width), BF16),
            sds((seqs, model_width), BF16),
            sds((seqs, peers), BF16),
            sds((seqs, width), F32),
        ),
        [SMEM] + [VMEM] * 7,
        [slab],
    )
    send, mid, pick, gate = middle(
        core, tokens, own, other, channel_gain.reshape(1, -1), expert_ids, expert_shares, branch_gate.reshape(1, -1)
    )
    arrived = lax.all_to_all(send, EP, 0, 0, tiled=True)
    down_other = pltpu.with_memory_space_constraint(down_other, pltpu.HBM)
    rows_out = call(
        experts_body,
        sds((peers, lines, width), BF16),
        [SMEM] + [VMEM] * 8 + [pl.BlockSpec(memory_space=pltpu.HBM)],
        [slab, pltpu.VMEM(expert_down.shape, BF16), pltpu.SemaphoreType.DMA(())],
    )(core, arrived, expert_gate, gate_other, expert_up, up_other, gathered, gathered_other, expert_down, down_other)
    returned = lax.all_to_all(rows_out, EP, 0, 0, tiled=True)
    keep, give = call(
        combine_body, (sds((seqs, half), F32), sds((seqs, half), F32)), [SMEM] + [VMEM] * 4, [slab]
    )(core, returned, pick, gate, mid)
    return (keep + swap(give, "tp")).astype(BF16)


def solution(mesh):
    torus = Mesh(mesh.devices.reshape(4, 2, 2, 2, 2, 2, 2), (*EP, "tp"))
    return jax.shard_map(
        layer,
        mesh=torus,
        in_specs=(
            P(EP, None),
            P(),
            P(None, "tp"),
            P(None, "tp"),
            P(None, "tp"),
            P("tp"),
            P(),
            P("tp", None),
            P(EP, None, "tp"),
            P(EP, None, "tp"),
            P(EP),
            P(),
            P(EP, None),
            P(EP, None),
            P(EP, None, "tp"),
            P(EP, None, "tp"),
            P(EP, "tp", None),
            P("tp", EP),
            P("tp", EP),
            P(EP, "tp"),
            P(),
        ),
        out_specs=P(EP, "tp"),
        check_vma=False,
    )
```

profile of v0, /device:TPU:1, one launch (start us, length us, event | category | flops | bytes accessed | tf_op | source)
XLA Modules:
  0.0 79.6 jit_solution(13496122344496054938)
XLA Ops:
  0.0 0.8 %maximum_bitcast_fusion = bf16[1,96,512]{2,1,0:T(8,128)(2,1)S(1)} fusion(bf16[32,512]{1,0:T(8,128)(2,1)} %param.40, bf16[32,512]{1,0:T(8,128)(2,1)} %bitcast.13, bf16[32,512]{1,0:T(8,128)(2,1)} %bitcast.15), kind=kLoop, calls=%fused_computation.1 | loop fusion | flops 294912 | bytes 196608 | tf_op jit(solution)/shard_map/broadcast_in_dim | solution.py:336
  0.8 2.5 %collective-permute-start.3 = (bf16[1,96,512]{2,1,0:T(8,128)(2,1)S(1)}, bf16[1,96,512]{2,1,0:T(8,128)(2,1)S(1)}, u32[]{:S(2)}, u32[]{:S(2)}) collective-permute-start(bf16[1,96,512]{2,1,0:T(8,128)(2,1)S(1)} %maximum_bitcast_fusion), channel_id=1, source_target_pairs={{0,32},{32,0},{1,33},{33,1},{2,34},{34,2},{3,35},{35,3},{4,36},{36... | collective-permute-start | bytes 294920 | tf_op jit(solution)/shard_map/ppermute | solution.py:317
  3.3 0.0 copy-start.9
  3.3 0.0 copy-start.10
  3.3 0.0 copy-start.6
  3.3 0.0 copy-start.7
  3.3 0.0 copy-start.8
  3.3 0.0 copy-start.3
  3.4 0.0 copy-start.4
  3.4 0.0 copy-start.5
  3.4 0.0 copy-start
  3.4 0.0 copy-start.1
  3.4 0.0 copy-start.2
  3.4 5.4 %attention.1.own = f32[16,1024]{1,0:T(8,128)S(1)} custom-call(s32[16]{0:T(128)} %lens_hbm.1, f32[4]{0:T(128)} %lam_hbm.1, bf16[16,1024]{1,0:T(8,128)(2,1)} %tokens.1, f32[1,1024]{1,0:T(1,128)} %bitcast.17, bf16[1024,512]{1,0:T(8,128)(2,1)} %wq_hbm.1, bf16[1024,128]{1,0:T(8,128)(2,1)} %wk_hbm.1, bf16[1024,128]{1,0:T(8,128)(2,1)} %wv_hbm.1, ...), custom_call_target="tpu_custom_call" | custom-call | flops 1000000000 | bytes 12582912 | tf_op jit(solution)/shard_map/attention/pallas_call | solution.py:158
  8.9 1.0 %collective-permute-start = (f32[16,1024]{1,0:T(8,128)S(1)}, f32[16,1024]{1,0:T(8,128)S(1)}, u32[]{:S(2)}, u32[]{:S(2)}) collective-permute-start(f32[16,1024]{1,0:T(8,128)S(1)} %attention.1.own), channel_id=1, source_target_pairs={{0,1},{1,0},{2,3},{3,2},{4,5},{5,4},{6,7},{7,6},{8,9},{9,8},{10,11... | collective-permute-start | bytes 196616 | tf_op jit(solution)/shard_map/ppermute | solution.py:317
  9.9 0.0 copy-done.9
  9.9 0.1 copy.22.ids
  10.0 0.0 copy-done.10
  10.0 0.1 copy.23.shares
  10.1 0.0 collective-permute-done.3
  10.1 1.4 %collective-permute-start.4 = (bf16[2,96,512]{2,1,0:T(8,128)(2,1)S(1)}, bf16[2,96,512]{2,1,0:T(8,128)(2,1)S(1)}, u32[]{:S(2)}, u32[]{:S(2)}) collective-permute-start(bf16[2,96,512]{2,1,0:T(8,128)(2,1)S(1)} %pad_maximum_fusion), channel_id=1, source_target_pairs={{0,8},{8,0},{1,9},{9,1},{2,10},{10,2},{3,11},{11,3},{4,12},{12,4},... | collective-permute-start | bytes 589832 | tf_op jit(solution)/shard_map/ppermute | solution.py:317
  11.5 1.2 %collective-permute-start.5 = (bf16[2,96,512]{2,1,0:T(8,128)(2,1)S(1)}, bf16[2,96,512]{2,1,0:T(8,128)(2,1)S(1)}, u32[]{:S(2)}, u32[]{:S(2)}) collective-permute-start(bf16[2,96,512]{2,1,0:T(8,128)(2,1)S(1)} %pad_maximum_fusion), channel_id=1, source_target_pairs={{0,2},{2,0},{1,3},{3,1},{4,6},{6,4},{5,7},{7,5},{8,10},{10,8},{9,1... | collective-permute-start | bytes 589832 | tf_op jit(solution)/shard_map/ppermute | solution.py:317
  12.7 0.0 copy-done.6
  12.7 0.0 copy-done.7
  12.7 0.0 copy-done.8
  12.7 0.0 collective-permute-done.other
  12.7 0.0 copy-done.3
  12.8 0.0 copy-done.4
  12.8 0.0 copy-done.5
  12.8 1.6 %shard_map.199 = (bf16[128,16,128]{2,1,0:T(8,128)(2,1)}, bf16[16,1024]{1,0:T(8,128)(2,1)S(1)}, bf16[16,128]{1,0:T(8,128)(2,1)S(1)}, f32[16,128]{1,0:T(8,128)S(1)}) custom-call(s32[1]{0:T(128)} %bitcast.core, bf16[16,1024]{1,0:T(8,128)(2,1)S(1)} %copy-done.3, f32[16,1024]{1,0:T(8,128)S(1)} %attention.1.own, f32[16,1024]{1,0:T(8,128)S(1)} %collective-permute-done.other, ...), custom_call_target="tpu_custom_call" | custom-call | flops 100000000 | bytes 2097152 | tf_op jit(solution)/shard_map/pallas_call | solution.py:362
  14.3 14.0 %all-to-all-start = ((bf16[128,16,128]{2,1,0:T(8,128)(2,1)}), bf16[128,16,128]{2,1,0:T(8,128)(2,1)S(1)}, u32[]{:S(2)}, u32[]{:S(2)}) async-start(bf16[128,16,128]{2,1,0:T(8,128)(2,1)} %get-tuple-element.11), calls=%async_computation | async-start | bytes 1048576 | tf_op jit(solution)/shard_map/all_to_all | solution.py:365
  28.4 0.0 collective-permute-done.4
  28.4 0.7 collective-permute-start.6
  29.1 0.0 collective-permute-done.5
  29.1 1.3 %collective-permute-start.7 = (bf16[1,96,512]{2,1,0:T(8,128)(2,1)S(1)}, bf16[1,96,512]{2,1,0:T(8,128)(2,1)S(1)}, u32[]{:S(2)}, u32[]{:S(2)}) collective-permute-start(bf16[1,96,512]{2,1,0:T(8,128)(2,1)S(1)} %slice.9), channel_id=1, source_target_pairs={{0,8},{8,0},{1,9},{9,1},{2,10},{10,2},{3,11},{11,3},{4,12},{12,4},... | collective-permute-start | bytes 294920 | tf_op jit(solution)/shard_map/ppermute | solution.py:317
  30.4 3.4 %collective-permute-done.6 = bf16[1,96,512]{2,1,0:T(8,128)(2,1)S(1)} collective-permute-done((bf16[1,96,512]{2,1,0:T(8,128)(2,1)S(1)}, bf16[1,96,512]{2,1,0:T(8,128)(2,1)S(1)}, u32[]{:S(2)}, u32[]{:S(2)}) %collective-permute-start.6) | collective-permute-done | bytes 98336 | tf_op jit(solution)/shard_map/ppermute | solution.py:317
  33.8 0.0 collective-permute-done.7
  33.9 2.1 %collective-permute-start.8 = (bf16[8,96,512]{2,1,0:T(8,128)(2,1)S(1)}, bf16[8,96,512]{2,1,0:T(8,128)(2,1)S(1)}, u32[]{:S(2)}, u32[]{:S(2)}) collective-permute-start(bf16[8,96,512]{2,1,0:T(8,128)(2,1)S(1)} %constant_dynamic-update-slice_fusion.dense_own), channel_id=1, source_target_pairs={{0,1},{1,0},{2,3},{3,2},{4,5},{5,4},{6,7},{7,6},{8,9},{9,8},{10,11... | collective-permute-start | bytes 2359304 | tf_op jit(solution)/shard_map/ppermute | solution.py:317
  36.0 0.0 copy-done
  36.0 0.1 collective-permute-start.1
  36.1 0.0 copy-done.1
  36.1 0.4 collective-permute-start.2
  36.5 0.0 copy-done.2
  36.5 0.3 collective-permute-start.9
  36.8 1.5 %collective-permute-done.1.gate_other = bf16[1,1024,128]{2,1,0:T(8,128)(2,1)S(1)} collective-permute-done((bf16[1,1024,128]{2,1,0:T(8,128)(2,1)S(1)}, bf16[1,1024,128]{2,1,0:T(8,128)(2,1)S(1)}, u32[]{:S(2)}, u32[]{:S(2)}) %collective-permute-start.1) | collective-permute-done | bytes 262176 | tf_op jit(solution)/shard_map/ppermute | solution.py:317
  38.3 0.4 collective-permute-done.2.up_other
  38.6 0.5 collective-permute-done.9.down_other
  39.2 7.8 %all-to-all-done.arrived = bf16[128,16,128]{2,1,0:T(8,128)(2,1)S(1)} async-done(((bf16[128,16,128]{2,1,0:T(8,128)(2,1)}), bf16[128,16,128]{2,1,0:T(8,128)(2,1)S(1)}, u32[]{:S(2)}, u32[]{:S(2)}) %all-to-all-start) | async-done | bytes 524320 | tf_op jit(solution)/shard_map/all_to_all | solution.py:365
  47.0 0.0 collective-permute-done.8.dense_other
  47.0 2.4 %shard_map.200 = bf16[128,16,128]{2,1,0:T(8,128)(2,1)S(1)} custom-call(s32[1]{0:T(128)} %bitcast.core, bf16[128,16,128]{2,1,0:T(8,128)(2,1)S(1)} %all-to-all-done.arrived, bf16[1,1024,128]{2,1,0:T(8,128)(2,1)S(1)} %copy-done, bf16[1,1024,128]{2,1,0:T(8,128)(2,1)S(1)} %collective-permute-done.1.gate_other, bf16[1,1024,128]{2,1,0:T(8,128)(2,1)S(1)} %copy-done.1, ...), custom_call_target="tpu_custom_call" | custom-call | flops 100000000 | bytes 2097152 | tf_op jit(solution)/shard_map/pallas_call | solution.py:367
  49.3 24.3 %all_to_all.10.returned = bf16[128,16,128]{2,1,0:T(8,128)(2,1)S(1)} all-to-all(bf16[128,16,128]{2,1,0:T(8,128)(2,1)S(1)} %shard_map.200), channel_id=1, replica_groups=mesh['zh'=4,'zl'=2,'yh'=2,'yl'=2,'xh'=2,'xl'=2,'tp'=2] {'zh','zl','yh','..., dimensions={0} | all-to-all | bytes 1048576 | tf_op jit(solution)/shard_map/all_to_all | solution.py:373
  73.6 0.5 shard_map.201
  74.1 4.0 %collective-permute-start.10 = (f32[16,512]{1,0:T(8,128)S(1)}, f32[16,512]{1,0:T(8,128)S(1)}, u32[]{:S(2)}, u32[]{:S(2)}) collective-permute-start(f32[16,512]{1,0:T(8,128)S(1)} %get-tuple-element.16), channel_id=1, source_target_pairs={{0,1},{1,0},{2,3},{3,2},{4,5},{5,4},{6,7},{7,6},{8,9},{9,8},{10,11... | collective-permute-start | bytes 98312 | tf_op jit(solution)/shard_map/ppermute | solution.py:317
  78.1 0.9 %collective-permute-done.10 = f32[16,512]{1,0:T(8,128)S(1)} collective-permute-done((f32[16,512]{1,0:T(8,128)S(1)}, f32[16,512]{1,0:T(8,128)S(1)}, u32[]{:S(2)}, u32[]{:S(2)}) %collective-permute-start.10) | collective-permute-done | bytes 32800 | tf_op jit(solution)/shard_map/ppermute | solution.py:317
  79.0 0.6 add_convert_fusion
  (9 shorter events, 0.1 us)
Async XLA Ops:
  0.8 9.3 %collective-permute-start.3 = (bf16[1,96,512]{2,1,0:T(8,128)(2,1)S(1)}, bf16[1,96,512]{2,1,0:T(8,128)(2,1)S(1)}, u32[]{:S(2)}, u32[]{:S(2)}) collective-permute-start(bf16[1,96,512]{2,1,0:T(8,128)(2,1)S(1)} %maximum_bitcast_fusion), channel_id=1, source_target_pairs={{0,32},{32,0},{1,33},{33,1},{2,34},{34,2},{3,35},{35,3},{4,36},{36... | collective-permute-start | bytes 294920 | tf_op jit(solution)/shard_map/ppermute | solution.py:317
  3.3 6.6 %copy-start.9 = (s32[16,6]{0,1:T(8,128)S(1)}, s32[16,6]{0,1:T(8,128)}, u32[]{:S(2)}) copy-start(s32[16,6]{0,1:T(8,128)} %param.33) | copy-start | bytes 1156
  3.3 6.7 %copy-start.10 = (bf16[16,6]{0,1:T(8,128)(2,1)S(1)}, bf16[16,6]{0,1:T(8,128)(2,1)}, u32[]{:S(2)}) copy-start(bf16[16,6]{0,1:T(8,128)(2,1)} %param.34) | copy-start | bytes 580
  3.3 9.4 %copy-start.6 = (bf16[32,512]{1,0:T(8,128)(2,1)S(1)}, bf16[32,512]{1,0:T(8,128)(2,1)}, u32[]{:S(2)}) copy-start(bf16[32,512]{1,0:T(8,128)(2,1)} %param.40) | copy-start | bytes 98308
  3.3 9.4 %copy-start.7 = (bf16[512,32]{0,1:T(8,128)(2,1)S(1)}, bf16[512,32]{0,1:T(8,128)(2,1)}, u32[]{:S(2)}) copy-start(bf16[512,32]{0,1:T(8,128)(2,1)} %param.39) | copy-start | bytes 98308
  3.3 9.4 %copy-start.8 = (bf16[512,32]{0,1:T(8,128)(2,1)S(1)}, bf16[512,32]{0,1:T(8,128)(2,1)}, u32[]{:S(2)}) copy-start(bf16[512,32]{0,1:T(8,128)(2,1)} %param.38) | copy-start | bytes 98308
  3.3 9.4 %copy-start.3 = (bf16[16,1024]{1,0:T(8,128)(2,1)S(1)}, bf16[16,1024]{1,0:T(8,128)(2,1)}, u32[]{:S(2)}) copy-start(bf16[16,1024]{1,0:T(8,128)(2,1)} %tokens.1) | copy-start | bytes 98308
  3.4 9.4 %copy-start.4 = (f32[1024]{0:T(1024)S(1)}, f32[1024]{0:T(1024)}, u32[]{:S(2)}) copy-start(f32[1024]{0:T(1024)} %param.32) | copy-start | bytes 12292
  3.4 9.4 %copy-start.5 = (f32[1024]{0:T(1024)S(1)}, f32[1024]{0:T(1024)}, u32[]{:S(2)}) copy-start(f32[1024]{0:T(1024)} %param.41) | copy-start | bytes 12292
  3.4 32.6 %copy-start = (bf16[1,1024,128]{2,1,0:T(8,128)(2,1)S(1)}, bf16[1,1024,128]{2,1,0:T(8,128)(2,1)}, u32[]{:S(2)}) copy-start(bf16[1,1024,128]{2,1,0:T(8,128)(2,1)} %gate_own.1) | copy-start | bytes 786436
  3.4 32.7 %copy-start.1 = (bf16[1,1024,128]{2,1,0:T(8,128)(2,1)S(1)}, bf16[1,1024,128]{2,1,0:T(8,128)(2,1)}, u32[]{:S(2)}) copy-start(bf16[1,1024,128]{2,1,0:T(8,128)(2,1)} %up_own.1) | copy-start | bytes 786436
  3.4 33.1 %copy-start.2 = (bf16[1,128,1024]{2,1,0:T(8,128)(2,1)S(1)}, bf16[1,128,1024]{2,1,0:T(8,128)(2,1)}, u32[]{:S(2)}) copy-start(bf16[1,128,1024]{2,1,0:T(8,128)(2,1)} %down_own.1) | copy-start | bytes 786436
  8.9 3.9 %collective-permute-start = (f32[16,1024]{1,0:T(8,128)S(1)}, f32[16,1024]{1,0:T(8,128)S(1)}, u32[]{:S(2)}, u32[]{:S(2)}) collective-permute-start(f32[16,1024]{1,0:T(8,128)S(1)} %attention.1.own), channel_id=1, source_target_pairs={{0,1},{1,0},{2,3},{3,2},{4,5},{5,4},{6,7},{7,6},{8,9},{9,8},{10,11... | collective-permute-start | bytes 196616 | tf_op jit(solution)/shard_map/ppermute | solution.py:317
  10.1 18.3 %collective-permute-start.4 = (bf16[2,96,512]{2,1,0:T(8,128)(2,1)S(1)}, bf16[2,96,512]{2,1,0:T(8,128)(2,1)S(1)}, u32[]{:S(2)}, u32[]{:S(2)}) collective-permute-start(bf16[2,96,512]{2,1,0:T(8,128)(2,1)S(1)} %pad_maximum_fusion), channel_id=1, source_target_pairs={{0,8},{8,0},{1,9},{9,1},{2,10},{10,2},{3,11},{11,3},{4,12},{12,4},... | collective-permute-start | bytes 589832 | tf_op jit(solution)/shard_map/ppermute | solution.py:317
  11.5 17.6 %collective-permute-start.5 = (bf16[2,96,512]{2,1,0:T(8,128)(2,1)S(1)}, bf16[2,96,512]{2,1,0:T(8,128)(2,1)S(1)}, u32[]{:S(2)}, u32[]{:S(2)}) collective-permute-start(bf16[2,96,512]{2,1,0:T(8,128)(2,1)S(1)} %pad_maximum_fusion), channel_id=1, source_target_pairs={{0,2},{2,0},{1,3},{3,1},{4,6},{6,4},{5,7},{7,5},{8,10},{10,8},{9,1... | collective-permute-start | bytes 589832 | tf_op jit(solution)/shard_map/ppermute | solution.py:317
  14.3 32.6 %all-to-all-start = ((bf16[128,16,128]{2,1,0:T(8,128)(2,1)}), bf16[128,16,128]{2,1,0:T(8,128)(2,1)S(1)}, u32[]{:S(2)}, u32[]{:S(2)}) async-start(bf16[128,16,128]{2,1,0:T(8,128)(2,1)} %get-tuple-element.11), calls=%async_computation | async-start | bytes 1048576 | tf_op jit(solution)/shard_map/all_to_all | solution.py:365
  28.4 5.4 %collective-permute-start.6 = (bf16[1,96,512]{2,1,0:T(8,128)(2,1)S(1)}, bf16[1,96,512]{2,1,0:T(8,128)(2,1)S(1)}, u32[]{:S(2)}, u32[]{:S(2)}) collective-permute-start(bf16[1,96,512]{2,1,0:T(8,128)(2,1)S(1)} %slice.8), channel_id=1, source_target_pairs={{0,2},{2,0},{1,3},{3,1},{4,6},{6,4},{5,7},{7,5},{8,10},{10,8},{9,1... | collective-permute-start | bytes 294920 | tf_op jit(solution)/shard_map/ppermute | solution.py:317
  29.1 4.8 %collective-permute-start.7 = (bf16[1,96,512]{2,1,0:T(8,128)(2,1)S(1)}, bf16[1,96,512]{2,1,0:T(8,128)(2,1)S(1)}, u32[]{:S(2)}, u32[]{:S(2)}) collective-permute-start(bf16[1,96,512]{2,1,0:T(8,128)(2,1)S(1)} %slice.9), channel_id=1, source_target_pairs={{0,8},{8,0},{1,9},{9,1},{2,10},{10,2},{3,11},{11,3},{4,12},{12,4},... | collective-permute-start | bytes 294920 | tf_op jit(solution)/shard_map/ppermute | solution.py:317
  33.9 13.1 %collective-permute-start.8 = (bf16[8,96,512]{2,1,0:T(8,128)(2,1)S(1)}, bf16[8,96,512]{2,1,0:T(8,128)(2,1)S(1)}, u32[]{:S(2)}, u32[]{:S(2)}) collective-permute-start(bf16[8,96,512]{2,1,0:T(8,128)(2,1)S(1)} %constant_dynamic-update-slice_fusion.dense_own), channel_id=1, source_target_pairs={{0,1},{1,0},{2,3},{3,2},{4,5},{5,4},{6,7},{7,6},{8,9},{9,8},{10,11... | collective-permute-start | bytes 2359304 | tf_op jit(solution)/shard_map/ppermute | solution.py:317
  36.0 2.3 %collective-permute-start.1 = (bf16[1,1024,128]{2,1,0:T(8,128)(2,1)S(1)}, bf16[1,1024,128]{2,1,0:T(8,128)(2,1)S(1)}, u32[]{:S(2)}, u32[]{:S(2)}) collective-permute-start(bf16[1,1024,128]{2,1,0:T(8,128)(2,1)S(1)} %copy-done), channel_id=1, source_target_pairs={{0,1},{1,0},{2,3},{3,2},{4,5},{5,4},{6,7},{7,6},{8,9},{9,8},{10,11... | collective-permute-start | bytes 786440 | tf_op jit(solution)/shard_map/ppermute | solution.py:317
  36.1 2.5 %collective-permute-start.2 = (bf16[1,1024,128]{2,1,0:T(8,128)(2,1)S(1)}, bf16[1,1024,128]{2,1,0:T(8,128)(2,1)S(1)}, u32[]{:S(2)}, u32[]{:S(2)}) collective-permute-start(bf16[1,1024,128]{2,1,0:T(8,128)(2,1)S(1)} %copy-done.1), channel_id=1, source_target_pairs={{0,1},{1,0},{2,3},{3,2},{4,5},{5,4},{6,7},{7,6},{8,9},{9,8},{10,11... | collective-permute-start | bytes 786440 | tf_op jit(solution)/shard_map/ppermute | solution.py:317
  36.5 2.6 %collective-permute-start.9 = (bf16[1,128,1024]{2,1,0:T(8,128)(2,1)S(1)}, bf16[1,128,1024]{2,1,0:T(8,128)(2,1)}, u32[]{:S(2)}, u32[]{:S(2)}) collective-permute-start(bf16[1,128,1024]{2,1,0:T(8,128)(2,1)S(1)} %copy-done.2), channel_id=1, source_target_pairs={{0,1},{1,0},{2,3},{3,2},{4,5},{5,4},{6,7},{7,6},{8,9},{9,8},{10,11... | collective-permute-start | bytes 786440 | tf_op jit(solution)/shard_map/ppermute | solution.py:317
  74.1 4.9 %collective-permute-start.10 = (f32[16,512]{1,0:T(8,128)S(1)}, f32[16,512]{1,0:T(8,128)S(1)}, u32[]{:S(2)}, u32[]{:S(2)}) collective-permute-start(f32[16,512]{1,0:T(8,128)S(1)} %get-tuple-element.16), channel_id=1, source_target_pairs={{0,1},{1,0},{2,3},{3,2},{4,5},{5,4},{6,7},{7,6},{8,9},{9,8},{10,11... | collective-permute-start | bytes 98312 | tf_op jit(solution)/shard_map/ppermute | solution.py:317
where the time goes:
time: 79.9 us; the launch traced here: 79.6 us
  starting transfers between devices  29 us (36%)
  blocking collectives  24.3 us (30%)
  waiting for transfers between devices  14.5 us (18%)
  Pallas kernels  9.84 us (12%)
  other arithmetic  1.44 us (2%)
    all_to_all x1, blocking collectives, layer(): returned = lax.all_to_all(rows_out, EP, 0, 0, tiled=True)  24.3 us
    ppermute x11, starting transfers between devices, swap(): return lax.ppermute(value, axis, [(0, 1), (1, 0)])  15 us
    all_to_all x1, starting transfers between devices, layer(): arrived = lax.all_to_all(send, EP, 0, 0, tiled=True)  14 us
    all_to_all x1, waiting for transfers between devices, layer(): arrived = lax.all_to_all(send, EP, 0, 0, tiled=True)  7.8 us
    ppermute x11, waiting for transfers between devices, swap(): return lax.ppermute(value, axis, [(0, 1), (1, 0)])  6.68 us
    pallas_call x1, Pallas kernels, attention(): pl.pallas_call(attention_body, out_shape=pltpu.VMEM((seqs, model_width),...  5.44 us
    pallas_call x1, Pallas kernels, layer(): call(experts_body, sds((peers, lines, width), BF16), [SMEM] + [VMEM] * 8...  2.37 us
  transfers between devices with their start and end apart: 12, of which 6 were waited for; matrix products, arithmetic and copies ran while one was open for 0% of the time, Pallas kernels for 9%

commit v1 on v0

--- a/solution.py
+++ b/solution.py
@@ -187,7 +187,6 @@
 
 
 EP = ("zh", "zl", "yh", "yl", "xh", "xl")
-SMEM = pl.BlockSpec(memory_space=pltpu.SMEM)
 VMEM = pl.BlockSpec(memory_space=pltpu.VMEM)
 
 
@@ -203,7 +202,7 @@
     )
 
 
-def mid_body(core, tokens, own, other, channel_gain, ids, shares, branch_gate, send, mid, pick, gate, slab):
+def mid_body(tokens, own, other, channel_gain, ids, shares, branch_gate, send, mid, pick, gate, slab):
     seqs, model_width = tokens.shape
     peers, lines, width = send.shape
     chunks = model_width // width
@@ -219,15 +218,17 @@
     row = lax.broadcasted_iota(jnp.int32, (seqs, peers), 0)
     share = jnp.zeros((seqs, peers), F32)
     picked = jnp.zeros((seqs, peers), F32)
-    for k in range(ids.shape[1]):
-        named = ids[:, k : k + 1] == peer
+    names, parts = jnp.transpose(ids[...].astype(F32)), jnp.transpose(shares[...].astype(F32))
+    peer_name = peer.astype(F32)
+    for k in range(ids.shape[0]):
+        named = names[:, k : k + 1] == peer_name
         picked = jnp.where(named, 1.0, picked)
-        share = jnp.where(named, shares[:, k : k + 1].astype(F32), share)
+        share = jnp.where(named, parts[:, k : k + 1], share)
     above = lax.broadcasted_iota(jnp.int32, (seqs, seqs), 0) >= lax.broadcasted_iota(jnp.int32, (seqs, seqs), 1)
     rank = jnp.dot(above.astype(BF16), picked.astype(BF16), preferred_element_type=F32)
-    placed = (picked > 0.0) & (rank == (core[0] + 1).astype(F32))
+    placed = (picked > 0.0) & (rank == (lax.axis_index("tp") + 1).astype(F32))
     pick[...] = jnp.where(placed, share, 0.0).astype(BF16)
-    dense = row == 2 * member(peer) + core[0]
+    dense = row == 2 * member(peer) + lax.axis_index("tp")
     for r, chosen in enumerate((placed, dense)):
         lines_out = lax.dot_general(
             chosen.astype(F32).astype(BF16), ffn, (((0,), (0,)), ((), ())), preferred_element_type=F32
@@ -247,7 +248,7 @@
 
 
 def experts_body(
-    core, arrived, gate_own, gate_other, up_own, up_other, dense_own, dense_other, down_own, down_other, out, slab,
+    arrived, gate_own, gate_other, up_own, up_other, dense_own, dense_other, down_own, down_other, out, slab,
     down_late, sem,
 ):
     late = pltpu.make_async_copy(down_other, down_late, sem)
@@ -258,7 +259,7 @@
     routed = jnp.concatenate(unpack(slab, 0, chunks, lines), axis=1)
     tokens = unpack(slab, chunks, chunks, lines)
     low, high = jnp.concatenate(tokens[: chunks // 2], axis=1), jnp.concatenate(tokens[chunks // 2 :], axis=1)
-    is_first = core[0] == 0
+    is_first = lax.axis_index("tp") == 0
     blocks, stacked, half_width = dense_own.shape
     units = stacked // 3
 
@@ -294,19 +295,19 @@
     out[...] = slab[...].reshape(out.shape).astype(BF16)
 
 
-def combine_body(core, returned, pick, gate, mid, keep, send, slab):
+def combine_body(returned, pick, gate, mid, keep, send, slab):
     peers, lines, width = returned.shape
     chunks = lines // 2
     seqs = pick.shape[0]
     slab[...] = returned[...].reshape(slab.shape).astype(F32)
     peer = lax.broadcasted_iota(jnp.int32, (seqs, peers), 1)
     row = lax.broadcasted_iota(jnp.int32, (seqs, peers), 0)
-    dense = (row == 2 * member(peer) + core[0]).astype(F32).astype(BF16)
+    dense = (row == 2 * member(peer) + lax.axis_index("tp")).astype(F32).astype(BF16)
     routed = jnp.dot(pick[...], jnp.concatenate(unpack(slab, 0, chunks, lines), axis=1), preferred_element_type=F32)
     branch = jnp.dot(dense, jnp.concatenate(unpack(slab, chunks, chunks, lines), axis=1), preferred_element_type=F32)
     total = routed + gate[:, :1] * branch
     half = chunks * width // 2
-    is_first = core[0] == 0
+    is_first = lax.axis_index("tp") == 0
     low, high = total[:, :half], total[:, half:]
     resid = mid[...].astype(F32)
     keep[...] = jnp.where(is_first, resid[:, :half] + low, resid[:, half:] + high)
@@ -327,7 +328,6 @@
     width = 2 * HD
     lines = 2 * model_width // width
     half = model_width // 2
-    core = lax.axis_index("tp").astype(jnp.int32).reshape(1)
     sds = jax.ShapeDtypeStruct
     slab = pltpu.VMEM((peers * lines, width), F32)
 
@@ -356,24 +356,24 @@
             sds((seqs, peers), BF16),
             sds((seqs, width), F32),
         ),
-        [SMEM] + [VMEM] * 7,
+        [VMEM] * 7,
         [slab],
     )
     send, mid, pick, gate = middle(
-        core, tokens, own, other, channel_gain.reshape(1, -1), expert_ids, expert_shares, branch_gate.reshape(1, -1)
+        tokens, own, other, channel_gain.reshape(1, -1), expert_ids.T, expert_shares.T, branch_gate.reshape(1, -1)
     )
     arrived = lax.all_to_all(send, EP, 0, 0, tiled=True)
     down_other = pltpu.with_memory_space_constraint(down_other, pltpu.HBM)
     rows_out = call(
         experts_body,
         sds((peers, lines, width), BF16),
-        [SMEM] + [VMEM] * 8 + [pl.BlockSpec(memory_space=pltpu.HBM)],
+        [VMEM] * 8 + [pl.BlockSpec(memory_space=pltpu.HBM)],
         [slab, pltpu.VMEM(expert_down.shape, BF16), pltpu.SemaphoreType.DMA(())],
-    )(core, arrived, expert_gate, gate_other, expert_up, up_other, gathered, gathered_other, expert_down, down_other)
+    )(arrived, expert_gate, gate_other, expert_up, up_other, gathered, gathered_other, expert_down, down_other)
     returned = lax.all_to_all(rows_out, EP, 0, 0, tiled=True)
     keep, give = call(
-        combine_body, (sds((seqs, half), F32), sds((seqs, half), F32)), [SMEM] + [VMEM] * 4, [slab]
-    )(core, returned, pick, gate, mid)
+        combine_body, (sds((seqs, half), F32), sds((seqs, half), F32)), [VMEM] * 4, [slab]
+    )(returned, pick, gate, mid)
     return (keep + swap(give, "tp")).astype(BF16)
 
 

time: 79.9 us -> 79.8 us (level)
  no operation moved by 1% of the time
where the time goes in v1:
time: 79.8 us; the launch traced here: 79.5 us
  starting transfers between devices  29 us (36%)
  blocking collectives  24.3 us (30%)
  waiting for transfers between devices  14.5 us (18%)
  Pallas kernels  9.93 us (12%)
  other arithmetic  1.44 us (2%)
    all_to_all x1, blocking collectives, layer(): returned = lax.all_to_all(rows_out, EP, 0, 0, tiled=True)  24.3 us
    ppermute x11, starting transfers between devices, swap(): return lax.ppermute(value, axis, [(0, 1), (1, 0)])  15 us
    all_to_all x1, starting transfers between devices, layer(): arrived = lax.all_to_all(send, EP, 0, 0, tiled=True)  14 us
    all_to_all x1, waiting for transfers between devices, layer(): arrived = lax.all_to_all(send, EP, 0, 0, tiled=True)  7.8 us
    ppermute x11, waiting for transfers between devices, swap(): return lax.ppermute(value, axis, [(0, 1), (1, 0)])  6.69 us
    pallas_call x1, Pallas kernels, attention(): pl.pallas_call(attention_body, out_shape=pltpu.VMEM((seqs, model_width),...  5.44 us
    pallas_call x1, Pallas kernels, layer(): call(experts_body, sds((peers, lines, width), BF16), [VMEM] * 8 + [pl.Blo...  2.37 us
    pallas_call x1, Pallas kernels, layer(): middle(tokens, own, other, channel_gain.reshape(1, -1), expert_ids.T, exp...  1.63 us
  transfers between devices with their start and end apart: 12, of which 6 were waited for; matrix products, arithmetic and copies ran while one was open for 0% of the time, Pallas kernels for 9%

profile of v1, /device:TPU:1, one launch (start us, length us, event | category | flops | bytes accessed | tf_op | source)
XLA Modules:
  0.0 79.5 jit_solution(13082844412994749209)
XLA Ops:
  0.0 0.8 %maximum_bitcast_fusion = bf16[1,96,512]{2,1,0:T(8,128)(2,1)S(1)} fusion(bf16[32,512]{1,0:T(8,128)(2,1)} %param.40, bf16[32,512]{1,0:T(8,128)(2,1)} %bitcast.16, bf16[32,512]{1,0:T(8,128)(2,1)} %bitcast.18), kind=kLoop, calls=%fused_computation.1 | loop fusion | flops 294912 | bytes 196608 | tf_op jit(solution)/shard_map/broadcast_in_dim | solution.py:336
  0.8 2.5 %collective-permute-start.3 = (bf16[1,96,512]{2,1,0:T(8,128)(2,1)S(1)}, bf16[1,96,512]{2,1,0:T(8,128)(2,1)S(1)}, u32[]{:S(2)}, u32[]{:S(2)}) collective-permute-start(bf16[1,96,512]{2,1,0:T(8,128)(2,1)S(1)} %maximum_bitcast_fusion), channel_id=1, source_target_pairs={{0,32},{32,0},{1,33},{33,1},{2,34},{34,2},{3,35},{35,3},{4,36},{36... | collective-permute-start | bytes 294920 | tf_op jit(solution)/shard_map/ppermute | solution.py:318
  3.3 0.0 copy-start.8
  3.3 0.0 copy-start.9
  3.3 0.0 copy-start.10
  3.3 0.0 copy-start.3
  3.3 0.0 copy-start.4
  3.3 0.0 copy-start.5
  3.4 0.0 copy-start.6
  3.4 0.0 copy-start.7
  3.4 0.0 copy-start
  3.4 0.0 copy-start.1
  3.4 0.0 copy-start.2
  3.4 5.4 %attention.1.own = f32[16,1024]{1,0:T(8,128)S(1)} custom-call(s32[16]{0:T(128)} %lens_hbm.1, f32[4]{0:T(128)} %lam_hbm.1, bf16[16,1024]{1,0:T(8,128)(2,1)} %tokens.1, f32[1,1024]{1,0:T(1,128)} %bitcast.20, bf16[1024,512]{1,0:T(8,128)(2,1)} %wq_hbm.1, bf16[1024,128]{1,0:T(8,128)(2,1)} %wk_hbm.1, bf16[1024,128]{1,0:T(8,128)(2,1)} %wv_hbm.1, ...), custom_call_target="tpu_custom_call" | custom-call | flops 1000000000 | bytes 12582912 | tf_op jit(solution)/shard_map/attention/pallas_call | solution.py:158
  8.9 1.0 %collective-permute-start = (f32[16,1024]{1,0:T(8,128)S(1)}, f32[16,1024]{1,0:T(8,128)S(1)}, u32[]{:S(2)}, u32[]{:S(2)}) collective-permute-start(f32[16,1024]{1,0:T(8,128)S(1)} %attention.1.own), channel_id=1, source_target_pairs={{0,1},{1,0},{2,3},{3,2},{4,5},{5,4},{6,7},{7,6},{8,9},{9,8},{10,11... | collective-permute-start | bytes 196616 | tf_op jit(solution)/shard_map/ppermute | solution.py:318
  9.9 0.0 collective-permute-done.3
  9.9 1.4 %collective-permute-start.4 = (bf16[2,96,512]{2,1,0:T(8,128)(2,1)S(1)}, bf16[2,96,512]{2,1,0:T(8,128)(2,1)S(1)}, u32[]{:S(2)}, u32[]{:S(2)}) collective-permute-start(bf16[2,96,512]{2,1,0:T(8,128)(2,1)S(1)} %pad_maximum_fusion), channel_id=1, source_target_pairs={{0,8},{8,0},{1,9},{9,1},{2,10},{10,2},{3,11},{11,3},{4,12},{12,4},... | collective-permute-start | bytes 589832 | tf_op jit(solution)/shard_map/ppermute | solution.py:318
  11.3 1.2 %collective-permute-start.5 = (bf16[2,96,512]{2,1,0:T(8,128)(2,1)S(1)}, bf16[2,96,512]{2,1,0:T(8,128)(2,1)S(1)}, u32[]{:S(2)}, u32[]{:S(2)}) collective-permute-start(bf16[2,96,512]{2,1,0:T(8,128)(2,1)S(1)} %pad_maximum_fusion), channel_id=1, source_target_pairs={{0,2},{2,0},{1,3},{3,1},{4,6},{6,4},{5,7},{7,5},{8,10},{10,8},{9,1... | collective-permute-start | bytes 589832 | tf_op jit(solution)/shard_map/ppermute | solution.py:318
  12.5 0.0 copy-done.8
  12.5 0.0 copy-done.9
  12.5 0.0 copy-done.10
  12.6 0.0 collective-permute-done.other
  12.6 0.0 copy-done.3
  12.6 0.0 copy-done.4
  12.6 0.0 copy-done.5
  12.6 0.0 copy-done.6
  12.6 0.0 copy-done.7
  12.6 1.6 %shard_map.199 = (bf16[128,16,128]{2,1,0:T(8,128)(2,1)}, bf16[16,1024]{1,0:T(8,128)(2,1)S(1)}, bf16[16,128]{1,0:T(8,128)(2,1)S(1)}, f32[16,128]{1,0:T(8,128)S(1)}) custom-call(bf16[16,1024]{1,0:T(8,128)(2,1)S(1)} %copy-done.3, f32[16,1024]{1,0:T(8,128)S(1)} %attention.1.own, f32[16,1024]{1,0:T(8,128)S(1)} %collective-permute-done.other, ...), custom_call_target="tpu_custom_call" | custom-call | flops 100000000 | bytes 2097152 | tf_op jit(solution)/shard_map/pallas_call | solution.py:362
  14.2 14.0 %all-to-all-start = ((bf16[128,16,128]{2,1,0:T(8,128)(2,1)}), bf16[128,16,128]{2,1,0:T(8,128)(2,1)S(1)}, u32[]{:S(2)}, u32[]{:S(2)}) async-start(bf16[128,16,128]{2,1,0:T(8,128)(2,1)} %get-tuple-element.11), calls=%async_computation | async-start | bytes 1048576 | tf_op jit(solution)/shard_map/all_to_all | solution.py:365
  28.3 0.0 collective-permute-done.4
  28.3 0.7 collective-permute-start.6
  29.0 0.0 collective-permute-done.5
  29.0 1.3 %collective-permute-start.7 = (bf16[1,96,512]{2,1,0:T(8,128)(2,1)S(1)}, bf16[1,96,512]{2,1,0:T(8,128)(2,1)S(1)}, u32[]{:S(2)}, u32[]{:S(2)}) collective-permute-start(bf16[1,96,512]{2,1,0:T(8,128)(2,1)S(1)} %slice.9), channel_id=1, source_target_pairs={{0,8},{8,0},{1,9},{9,1},{2,10},{10,2},{3,11},{11,3},{4,12},{12,4},... | collective-permute-start | bytes 294920 | tf_op jit(solution)/shard_map/ppermute | solution.py:318
  30.3 3.4 %collective-permute-done.6 = bf16[1,96,512]{2,1,0:T(8,128)(2,1)S(1)} collective-permute-done((bf16[1,96,512]{2,1,0:T(8,128)(2,1)S(1)}, bf16[1,96,512]{2,1,0:T(8,128)(2,1)S(1)}, u32[]{:S(2)}, u32[]{:S(2)}) %collective-permute-start.6) | collective-permute-done | bytes 98336 | tf_op jit(solution)/shard_map/ppermute | solution.py:318
  33.7 0.0 collective-permute-done.7
  33.8 2.1 %collective-permute-start.8 = (bf16[8,96,512]{2,1,0:T(8,128)(2,1)S(1)}, bf16[8,96,512]{2,1,0:T(8,128)(2,1)S(1)}, u32[]{:S(2)}, u32[]{:S(2)}) collective-permute-start(bf16[8,96,512]{2,1,0:T(8,128)(2,1)S(1)} %constant_dynamic-update-slice_fusion.dense_own), channel_id=1, source_target_pairs={{0,1},{1,0},{2,3},{3,2},{4,5},{5,4},{6,7},{7,6},{8,9},{9,8},{10,11... | collective-permute-start | bytes 2359304 | tf_op jit(solution)/shard_map/ppermute | solution.py:318
  35.9 0.0 copy-done
  35.9 0.1 collective-permute-start.1
  36.0 0.0 copy-done.1
  36.0 0.4 collective-permute-start.2
  36.4 0.0 copy-done.2
  36.4 0.3 collective-permute-start.9
  36.7 1.5 %collective-permute-done.1.gate_other = bf16[1,1024,128]{2,1,0:T(8,128)(2,1)S(1)} collective-permute-done((bf16[1,1024,128]{2,1,0:T(8,128)(2,1)S(1)}, bf16[1,1024,128]{2,1,0:T(8,128)(2,1)S(1)}, u32[]{:S(2)}, u32[]{:S(2)}) %collective-permute-start.1) | collective-permute-done | bytes 262176 | tf_op jit(solution)/shard_map/ppermute | solution.py:318
  38.2 0.4 collective-permute-done.2.up_other
  38.5 0.5 collective-permute-done.9.down_other
  39.0 7.8 %all-to-all-done.arrived = bf16[128,16,128]{2,1,0:T(8,128)(2,1)S(1)} async-done(((bf16[128,16,128]{2,1,0:T(8,128)(2,1)}), bf16[128,16,128]{2,1,0:T(8,128)(2,1)S(1)}, u32[]{:S(2)}, u32[]{:S(2)}) %all-to-all-start) | async-done | bytes 524320 | tf_op jit(solution)/shard_map/all_to_all | solution.py:365
  46.9 0.0 collective-permute-done.8.dense_other
  46.9 2.4 %shard_map.200 = bf16[128,16,128]{2,1,0:T(8,128)(2,1)S(1)} custom-call(bf16[128,16,128]{2,1,0:T(8,128)(2,1)S(1)} %all-to-all-done.arrived, bf16[1,1024,128]{2,1,0:T(8,128)(2,1)S(1)} %copy-done, bf16[1,1024,128]{2,1,0:T(8,128)(2,1)S(1)} %collective-permute-done.1.gate_other, bf16[1,1024,128]{2,1,0:T(8,128)(2,1)S(1)} %copy-done.1, ...), custom_call_target="tpu_custom_call" | custom-call | flops 100000000 | bytes 2097152 | tf_op jit(solution)/shard_map/pallas_call | solution.py:367
  49.2 24.3 %all_to_all.10.returned = bf16[128,16,128]{2,1,0:T(8,128)(2,1)S(1)} all-to-all(bf16[128,16,128]{2,1,0:T(8,128)(2,1)S(1)} %shard_map.200), channel_id=1, replica_groups=mesh['zh'=4,'zl'=2,'yh'=2,'yl'=2,'xh'=2,'xl'=2,'tp'=2] {'zh','zl','yh','..., dimensions={0} | all-to-all | bytes 1048576 | tf_op jit(solution)/shard_map/all_to_all | solution.py:373
  73.5 0.5 shard_map.201
  74.0 4.0 %collective-permute-start.10 = (f32[16,512]{1,0:T(8,128)S(1)}, f32[16,512]{1,0:T(8,128)S(1)}, u32[]{:S(2)}, u32[]{:S(2)}) collective-permute-start(f32[16,512]{1,0:T(8,128)S(1)} %get-tuple-element.16), channel_id=1, source_target_pairs={{0,1},{1,0},{2,3},{3,2},{4,5},{5,4},{6,7},{7,6},{8,9},{9,8},{10,11... | collective-permute-start | bytes 98312 | tf_op jit(solution)/shard_map/ppermute | solution.py:318
  78.0 0.9 %collective-permute-done.10 = f32[16,512]{1,0:T(8,128)S(1)} collective-permute-done((f32[16,512]{1,0:T(8,128)S(1)}, f32[16,512]{1,0:T(8,128)S(1)}, u32[]{:S(2)}, u32[]{:S(2)}) %collective-permute-start.10) | collective-permute-done | bytes 32800 | tf_op jit(solution)/shard_map/ppermute | solution.py:318
  78.9 0.6 add_convert_fusion
  (9 shorter events, 0.1 us)
Async XLA Ops:
  0.8 9.1 %collective-permute-start.3 = (bf16[1,96,512]{2,1,0:T(8,128)(2,1)S(1)}, bf16[1,96,512]{2,1,0:T(8,128)(2,1)S(1)}, u32[]{:S(2)}, u32[]{:S(2)}) collective-permute-start(bf16[1,96,512]{2,1,0:T(8,128)(2,1)S(1)} %maximum_bitcast_fusion), channel_id=1, source_target_pairs={{0,32},{32,0},{1,33},{33,1},{2,34},{34,2},{3,35},{35,3},{4,36},{36... | collective-permute-start | bytes 294920 | tf_op jit(solution)/shard_map/ppermute | solution.py:318
  3.3 9.2 %copy-start.8 = (bf16[32,512]{1,0:T(8,128)(2,1)S(1)}, bf16[32,512]{1,0:T(8,128)(2,1)}, u32[]{:S(2)}) copy-start(bf16[32,512]{1,0:T(8,128)(2,1)} %param.40) | copy-start | bytes 98308
  3.3 9.2 %copy-start.9 = (bf16[512,32]{0,1:T(8,128)(2,1)S(1)}, bf16[512,32]{0,1:T(8,128)(2,1)}, u32[]{:S(2)}) copy-start(bf16[512,32]{0,1:T(8,128)(2,1)} %param.39) | copy-start | bytes 98308
  3.3 9.2 %copy-start.10 = (bf16[512,32]{0,1:T(8,128)(2,1)S(1)}, bf16[512,32]{0,1:T(8,128)(2,1)}, u32[]{:S(2)}) copy-start(bf16[512,32]{0,1:T(8,128)(2,1)} %param.38) | copy-start | bytes 98308
  3.3 9.2 %copy-start.3 = (bf16[16,1024]{1,0:T(8,128)(2,1)S(1)}, bf16[16,1024]{1,0:T(8,128)(2,1)}, u32[]{:S(2)}) copy-start(bf16[16,1024]{1,0:T(8,128)(2,1)} %tokens.1) | copy-start | bytes 98308
  3.3 9.2 %copy-start.4 = (f32[1024]{0:T(1024)S(1)}, f32[1024]{0:T(1024)}, u32[]{:S(2)}) copy-start(f32[1024]{0:T(1024)} %param.32) | copy-start | bytes 12292
  3.3 9.2 %copy-start.5 = (s32[16,6]{0,1:T(8,128)S(1)}, s32[16,6]{0,1:T(8,128)}, u32[]{:S(2)}) copy-start(s32[16,6]{0,1:T(8,128)} %param.33) | copy-start | bytes 1156
  3.4 9.2 %copy-start.6 = (f32[1024]{0:T(1024)S(1)}, f32[1024]{0:T(1024)}, u32[]{:S(2)}) copy-start(f32[1024]{0:T(1024)} %param.41) | copy-start | bytes 12292
  3.4 9.2 %copy-start.7 = (bf16[16,6]{0,1:T(8,128)(2,1)S(1)}, bf16[16,6]{0,1:T(8,128)(2,1)}, u32[]{:S(2)}) copy-start(bf16[16,6]{0,1:T(8,128)(2,1)} %param.34) | copy-start | bytes 580
  3.4 32.5 %copy-start = (bf16[1,1024,128]{2,1,0:T(8,128)(2,1)S(1)}, bf16[1,1024,128]{2,1,0:T(8,128)(2,1)}, u32[]{:S(2)}) copy-start(bf16[1,1024,128]{2,1,0:T(8,128)(2,1)} %gate_own.1) | copy-start | bytes 786436
  3.4 32.6 %copy-start.1 = (bf16[1,1024,128]{2,1,0:T(8,128)(2,1)S(1)}, bf16[1,1024,128]{2,1,0:T(8,128)(2,1)}, u32[]{:S(2)}) copy-start(bf16[1,1024,128]{2,1,0:T(8,128)(2,1)} %up_own.1) | copy-start | bytes 786436
  3.4 33.0 %copy-start.2 = (bf16[1,128,1024]{2,1,0:T(8,128)(2,1)S(1)}, bf16[1,128,1024]{2,1,0:T(8,128)(2,1)}, u32[]{:S(2)}) copy-start(bf16[1,128,1024]{2,1,0:T(8,128)(2,1)} %down_own.1) | copy-start | bytes 786436
  8.9 3.7 %collective-permute-start = (f32[16,1024]{1,0:T(8,128)S(1)}, f32[16,1024]{1,0:T(8,128)S(1)}, u32[]{:S(2)}, u32[]{:S(2)}) collective-permute-start(f32[16,1024]{1,0:T(8,128)S(1)} %attention.1.own), channel_id=1, source_target_pairs={{0,1},{1,0},{2,3},{3,2},{4,5},{5,4},{6,7},{7,6},{8,9},{9,8},{10,11... | collective-permute-start | bytes 196616 | tf_op jit(solution)/shard_map/ppermute | solution.py:318
  9.9 18.4 %collective-permute-start.4 = (bf16[2,96,512]{2,1,0:T(8,128)(2,1)S(1)}, bf16[2,96,512]{2,1,0:T(8,128)(2,1)S(1)}, u32[]{:S(2)}, u32[]{:S(2)}) collective-permute-start(bf16[2,96,512]{2,1,0:T(8,128)(2,1)S(1)} %pad_maximum_fusion), channel_id=1, source_target_pairs={{0,8},{8,0},{1,9},{9,1},{2,10},{10,2},{3,11},{11,3},{4,12},{12,4},... | collective-permute-start | bytes 589832 | tf_op jit(solution)/shard_map/ppermute | solution.py:318
  11.3 17.7 %collective-permute-start.5 = (bf16[2,96,512]{2,1,0:T(8,128)(2,1)S(1)}, bf16[2,96,512]{2,1,0:T(8,128)(2,1)S(1)}, u32[]{:S(2)}, u32[]{:S(2)}) collective-permute-start(bf16[2,96,512]{2,1,0:T(8,128)(2,1)S(1)} %pad_maximum_fusion), channel_id=1, source_target_pairs={{0,2},{2,0},{1,3},{3,1},{4,6},{6,4},{5,7},{7,5},{8,10},{10,8},{9,1... | collective-permute-start | bytes 589832 | tf_op jit(solution)/shard_map/ppermute | solution.py:318
  14.2 32.6 %all-to-all-start = ((bf16[128,16,128]{2,1,0:T(8,128)(2,1)}), bf16[128,16,128]{2,1,0:T(8,128)(2,1)S(1)}, u32[]{:S(2)}, u32[]{:S(2)}) async-start(bf16[128,16,128]{2,1,0:T(8,128)(2,1)} %get-tuple-element.11), calls=%async_computation | async-start | bytes 1048576 | tf_op jit(solution)/shard_map/all_to_all | solution.py:365
  28.3 5.4 %collective-permute-start.6 = (bf16[1,96,512]{2,1,0:T(8,128)(2,1)S(1)}, bf16[1,96,512]{2,1,0:T(8,128)(2,1)S(1)}, u32[]{:S(2)}, u32[]{:S(2)}) collective-permute-start(bf16[1,96,512]{2,1,0:T(8,128)(2,1)S(1)} %slice.8), channel_id=1, source_target_pairs={{0,2},{2,0},{1,3},{3,1},{4,6},{6,4},{5,7},{7,5},{8,10},{10,8},{9,1... | collective-permute-start | bytes 294920 | tf_op jit(solution)/shard_map/ppermute | solution.py:318
  29.0 4.8 %collective-permute-start.7 = (bf16[1,96,512]{2,1,0:T(8,128)(2,1)S(1)}, bf16[1,96,512]{2,1,0:T(8,128)(2,1)S(1)}, u32[]{:S(2)}, u32[]{:S(2)}) collective-permute-start(bf16[1,96,512]{2,1,0:T(8,128)(2,1)S(1)} %slice.9), channel_id=1, source_target_pairs={{0,8},{8,0},{1,9},{9,1},{2,10},{10,2},{3,11},{11,3},{4,12},{12,4},... | collective-permute-start | bytes 294920 | tf_op jit(solution)/shard_map/ppermute | solution.py:318
  33.8 13.1 %collective-permute-start.8 = (bf16[8,96,512]{2,1,0:T(8,128)(2,1)S(1)}, bf16[8,96,512]{2,1,0:T(8,128)(2,1)S(1)}, u32[]{:S(2)}, u32[]{:S(2)}) collective-permute-start(bf16[8,96,512]{2,1,0:T(8,128)(2,1)S(1)} %constant_dynamic-update-slice_fusion.dense_own), channel_id=1, source_target_pairs={{0,1},{1,0},{2,3},{3,2},{4,5},{5,4},{6,7},{7,6},{8,9},{9,8},{10,11... | collective-permute-start | bytes 2359304 | tf_op jit(solution)/shard_map/ppermute | solution.py:318
  35.9 2.3 %collective-permute-start.1 = (bf16[1,1024,128]{2,1,0:T(8,128)(2,1)S(1)}, bf16[1,1024,128]{2,1,0:T(8,128)(2,1)S(1)}, u32[]{:S(2)}, u32[]{:S(2)}) collective-permute-start(bf16[1,1024,128]{2,1,0:T(8,128)(2,1)S(1)} %copy-done), channel_id=1, source_target_pairs={{0,1},{1,0},{2,3},{3,2},{4,5},{5,4},{6,7},{7,6},{8,9},{9,8},{10,11... | collective-permute-start | bytes 786440 | tf_op jit(solution)/shard_map/ppermute | solution.py:318
  36.0 2.5 %collective-permute-start.2 = (bf16[1,1024,128]{2,1,0:T(8,128)(2,1)S(1)}, bf16[1,1024,128]{2,1,0:T(8,128)(2,1)S(1)}, u32[]{:S(2)}, u32[]{:S(2)}) collective-permute-start(bf16[1,1024,128]{2,1,0:T(8,128)(2,1)S(1)} %copy-done.1), channel_id=1, source_target_pairs={{0,1},{1,0},{2,3},{3,2},{4,5},{5,4},{6,7},{7,6},{8,9},{9,8},{10,11... | collective-permute-start | bytes 786440 | tf_op jit(solution)/shard_map/ppermute | solution.py:318
  36.4 2.6 %collective-permute-start.9 = (bf16[1,128,1024]{2,1,0:T(8,128)(2,1)S(1)}, bf16[1,128,1024]{2,1,0:T(8,128)(2,1)}, u32[]{:S(2)}, u32[]{:S(2)}) collective-permute-start(bf16[1,128,1024]{2,1,0:T(8,128)(2,1)S(1)} %copy-done.2), channel_id=1, source_target_pairs={{0,1},{1,0},{2,3},{3,2},{4,5},{5,4},{6,7},{7,6},{8,9},{9,8},{10,11... | collective-permute-start | bytes 786440 | tf_op jit(solution)/shard_map/ppermute | solution.py:318
  74.0 4.9 %collective-permute-start.10 = (f32[16,512]{1,0:T(8,128)S(1)}, f32[16,512]{1,0:T(8,128)S(1)}, u32[]{:S(2)}, u32[]{:S(2)}) collective-permute-start(f32[16,512]{1,0:T(8,128)S(1)} %get-tuple-element.16), channel_id=1, source_target_pairs={{0,1},{1,0},{2,3},{3,2},{4,5},{5,4},{6,7},{7,6},{8,9},{9,8},{10,11... | collective-permute-start | bytes 98312 | tf_op jit(solution)/shard_map/ppermute | solution.py:318
